TPU v7x, 32 devices: a whole 2x2x4 slice. The times are simulated.
32 devices in a mesh: grp: 2 (over x), tp: 4 (over y, core), dp: 4 (over z).
Axes of the slice: x: 2, y: 2, z: 4, core: 2. Of those that a mesh axis runs over, the one named last changes fastest.
Arguments:
- tokens: bfloat16 [64, 4096], P(('grp', 'tp'), 'dp'), parts along dimension 0, may hold values from -45 to 45
- w_in: bfloat16 [2, 2, 4096, 8192], P(None, None, 'dp', 'tp'), may hold values from -0.09375 to 0.09375
- w_vec: bfloat16 [2, 2, 4096, 2048], P(None, None, 'dp', 'tp'), may hold values from -0.09375 to 0.09375
- w_step: bfloat16 [2, 4096, 128], P(None, 'dp'), may hold values from -0.09375 to 0.09375
- conv_weight: bfloat16 [2, 4, 8192], P(None, None, 'tp'), may hold values from -3 to 3
- conv_vec: bfloat16 [2, 2, 4, 2048], P(None, None, None, 'tp'), may hold values from -3 to 3
- conv_state: bfloat16 [2, 64, 3, 8192], P(None, ('grp', 'dp'), None, 'tp'), parts along dimension 1, may hold values from -6 to 6
- vec_state: bfloat16 [2, 2, 64, 3, 2048], P(None, None, ('grp', 'dp'), None, 'tp'), parts along dimension 2, may hold values from -6 to 6
- ssm_state: float32 [2, 64, 128, 64, 128], P(None, ('grp', 'dp'), 'tp'), parts along dimension 1, may hold values from -4 to 4
- step_bias: float32 [2, 128], P(None, 'tp'), may hold values from -1.5 to 1
- decay_log: float32 [2, 128], P(None, 'tp'), may hold values from -4 to 1
- skip_gain: float32 [2, 128], P(None, 'tp'), may hold values from 0.5 to 3
- mix_gain: bfloat16 [2, 4096], P(None, 'dp'), may hold values from 0.099609375 to 1.8984375
- out_gain: bfloat16 [2, 8192], P(None, 'tp'), may hold values from 0.099609375 to 1.8984375
- w_out: bfloat16 [2, 8192, 4096], P(None, 'tp', 'dp'), may hold values from -0.0625 to 0.0625
Outputs:
- new_tokens: bfloat16 [64, 4096], P(('grp', 'tp'), 'dp'), parts along dimension 0
- new_conv: bfloat16 [2, 64, 3, 8192], P(None, ('grp', 'dp'), None, 'tp'), parts along dimension 1
- new_vec: bfloat16 [2, 2, 64, 3, 2048], P(None, None, ('grp', 'dp'), None, 'tp'), parts along dimension 2
- new_ssm: float32 [2, 64, 128, 64, 128], P(None, ('grp', 'dp'), 'tp'), parts along dimension 1
There are 2 independent parts, one for each index of `grp`. A program takes and returns all parts, laid end to end along the dimension named above; an argument that names none is the same for every part. Nothing has to cross between parts.
All inputs are finite; a program needn't handle non-finite values.
Results may differ from a plain program's by a relative error of at most 0.023.
Values may be sent and summed in bfloat16 or wider, within the bound.
A program may use at most 128 MiB of HBM per device.

v0:
```python
import jax
import jax.numpy as jnp
from jax import lax
from jax.sharding import PartitionSpec as P

MODEL_WIDTH = 4096
HEAD_COUNT = 128
HEAD_DIM = 64
STATE_DIM = 128
GROUP_COUNT = 16
LAYER_COUNT = 2


EPS = 1e-06


def mixer_step(
    current,
    layer,
    w_in,
    w_vec,
    w_step,
    conv_weight,
    conv_vec,
    conv_state,
    vec_state,
    ssm_state,
    step_bias,
    decay_log,
    skip_gain,
    mix_gain,
    out_gain,
    w_out,
):
    whole_rows = lax.all_gather(current, "tp", axis=0, tiled=True)
    xf = whole_rows.astype(jnp.float32)
    squares = jnp.sum(xf * xf, axis=1)
    scaled_in = (xf * mix_gain[layer].astype(jnp.float32)).astype(jnp.bfloat16)
    step_part = jnp.dot(scaled_in, w_step[layer], preferred_element_type=jnp.float32)
    proj_part = jnp.einsum(
        "bd,rdc->brc", scaled_in, w_in[layer], preferred_element_type=jnp.float32
    )
    proj_sum = lax.psum_scatter(
        proj_part.astype(jnp.bfloat16), "dp", scatter_dimension=0, tiled=True
    ).astype(jnp.float32)
    vec_part = jnp.einsum(
        "bd,rdc->brc", scaled_in, w_vec[layer], preferred_element_type=jnp.float32
    )
    vec_total, step_sum, own_sq = (
        lax.psum_scatter(
            vec_part.astype(jnp.bfloat16), "dp", scatter_dimension=0, tiled=True
        ).astype(jnp.float32),
        lax.psum_scatter(
            step_part.astype(jnp.bfloat16), "dp", scatter_dimension=0, tiled=True
        ).astype(jnp.float32),
        lax.psum_scatter(
            squares.astype(jnp.bfloat16), "dp", scatter_dimension=0, tiled=True
        ).astype(jnp.float32),
    )
    local_rows = proj_sum.shape[0]
    columns = proj_sum.shape[2]
    vec_columns = vec_total.shape[2]
    scale = lax.rsqrt(own_sq / MODEL_WIDTH + EPS)
    proj = (proj_sum * scale[:, None, None]).astype(jnp.bfloat16)
    vecs = (vec_total * scale[:, None, None]).astype(jnp.bfloat16)
    local_heads = ssm_state.shape[2]
    head_start = lax.axis_index("tp") * local_heads
    step_raw = lax.dynamic_slice_in_dim(step_sum, head_start, local_heads, 1) * scale[:, None]
    window = jnp.concatenate([conv_state[layer], proj[:, 1][:, None, :]], axis=1)
    new_conv = window[:, 1:, :]
    values_sum = jnp.sum(
        window.astype(jnp.float32) * conv_weight[layer].astype(jnp.float32)[None, :, :], axis=1
    )
    fresh = jnp.transpose(vecs, (1, 0, 2))[:, :, None, :]
    vec_window = jnp.concatenate([vec_state[layer], fresh], axis=2)
    new_vec = vec_window[:, :, 1:, :]
    vec_sum = jnp.sum(
        vec_window.astype(jnp.float32) * conv_vec[layer].astype(jnp.float32)[:, None, :, :], axis=2
    )
    values = jax.nn.silu(values_sum).reshape(local_rows, local_heads, HEAD_DIM)
    vec_act = jax.nn.silu(vec_sum)
    local_groups = vec_columns // STATE_DIM
    repeat = HEAD_COUNT // GROUP_COUNT
    in_vec = jnp.repeat(vec_act[0].reshape(local_rows, local_groups, STATE_DIM), repeat, axis=1)
    out_vec = jnp.repeat(vec_act[1].reshape(local_rows, local_groups, STATE_DIM), repeat, axis=1)
    step = jax.nn.softplus(step_raw + step_bias[layer][None, :])
    decay = jnp.exp(-step * jnp.exp(decay_log[layer])[None, :])
    state = (
        decay[:, :, None, None] * ssm_state[layer]
        + (step[:, :, None] * values)[..., None] * in_vec[:, :, None, :]
    )
    read = jnp.einsum("bhpn,bhn->bhp", state, out_vec) + skip_gain[layer][None, :, None] * values
    mixed = read.reshape(local_rows, columns) * jax.nn.silu(proj[:, 0].astype(jnp.float32))
    grouped = mixed.reshape(local_rows, local_groups, columns // local_groups)
    grouped = grouped * lax.rsqrt(jnp.mean(grouped * grouped, axis=2, keepdims=True) + EPS)
    normed = (grouped.reshape(local_rows, columns) * out_gain[layer].astype(jnp.float32)).astype(
        jnp.bfloat16
    )
    out_weight = w_out[layer]
    out_terms = jnp.dot(
        lax.all_gather(normed, "dp", axis=0, tiled=True),
        out_weight,
        preferred_element_type=jnp.float32,
    )
    out_sum = lax.psum_scatter(
        out_terms.astype(jnp.bfloat16), "tp", scatter_dimension=0, tiled=True
    ).astype(jnp.float32)
    result = (current.astype(jnp.float32) + out_sum).astype(jnp.bfloat16)
    return (result, new_conv, new_vec, state)


def shards(
    tokens,
    w_in,
    w_vec,
    w_step,
    conv_weight,
    conv_vec,
    conv_state,
    vec_state,
    ssm_state,
    step_bias,
    decay_log,
    skip_gain,
    mix_gain,
    out_gain,
    w_out,
):
    current = tokens
    convs = []
    vec_rows = []
    states = []
    for layer in range(LAYER_COUNT):
        current, conv_next, vec_next, state_next = mixer_step(
            current,
            layer,
            w_in,
            w_vec,
            w_step,
            conv_weight,
            conv_vec,
            conv_state,
            vec_state,
            ssm_state,
            step_bias,
            decay_log,
            skip_gain,
            mix_gain,
            out_gain,
            w_out,
        )
        convs.append(conv_next)
        vec_rows.append(vec_next)
        states.append(state_next)
    return (current, jnp.stack(convs), jnp.stack(vec_rows), jnp.stack(states))


def solution(mesh):
    placed = (
        P(("grp", "tp"), "dp"),
        P(None, None, "dp", "tp"),
        P(None, None, "dp", "tp"),
        P(None, "dp", None),
        P(None, None, "tp"),
        P(None, None, None, "tp"),
        P(None, ("grp", "dp"), None, "tp"),
        P(None, None, ("grp", "dp"), None, "tp"),
        P(None, ("grp", "dp"), "tp", None, None),
        P(None, "tp"),
        P(None, "tp"),
        P(None, "tp"),
        P(None, "dp"),
        P(None, "tp"),
        P(None, "tp", "dp"),
    )
    return jax.shard_map(
        shards,
        mesh=mesh,
        in_specs=placed,
        out_specs=(
            P(("grp", "tp"), "dp"),
            P(None, ("grp", "dp"), None, "tp"),
            P(None, None, ("grp", "dp"), None, "tp"),
            P(None, ("grp", "dp"), "tp", None, None),
        ),
        check_vma=False,
    )
```

profile of v0, /device:TPU:0, one launch (start us, length us, event | category | flops | bytes accessed | tf_op | source)
XLA Modules:
  0.0 220.2 jit_solution(17541386348252600934)
XLA Ops:
  8.1 6.5 %all_gather.12 = bf16[32,1024]{1,0:T(8,128)(2,1)S(1)} all-gather(bf16[8,1024]{1,0:T(8,128)(2,1)} %param.15), channel_id=1, replica_groups=mesh['grp'=2,'tp'=4,'dp'=4] {'tp'}, dimensions={0}, use_global_device_ids=true | all-gather | bytes 81920 | tf_op jit(solution)/shard_map/all_gather | solution.py:35
  14.6 2.0 fusion.61
  17.3 4.9 %fusion.37 = bf16[2,4,8,2048]{3,2,1,0:T(8,128)(2,1)S(1)} fusion(bf16[2,2,1024,2048]{3,2,1,0:T(8,128)(2,1)} %param.16, bf16[32,1024]{1,0:T(8,128)(2,1)S(1)} %all_gather.12, f32[1024]{0:T(1024)S(1)} %bitcast.231), kind=kOutput, calls=%fused_computation.34 | convolution fusion | flops 268664832 | bytes 8720384 | tf_op jit(solution)/shard_map/bd,rdc->brc/dot_general | solution.py:40
  24.7 12.9 %all-reduce.5 = (bf16[32]{0:T(256)(128)(2,1)S(1)}, bf16[32,128]{1,0:T(8,128)(2,1)S(1)}) all-reduce(bf16[32]{0:T(256)(128)(2,1)S(1)} %fusion.69, bf16[32,128]{1,0:T(8,128)(2,1)S(1)} %convolution_convert_fusion.1), channel_id=3, replica_groups=mesh['grp'=2,'tp'=4,'dp'=4] {'dp'}, use_global_device_ids=true, to_apply=%region_2.0.clone | all-reduce | flops 4128 | bytes 16512
  39.3 20.2 %reduce-scatter.19.cloned.1.call-done = bf16[8,4096]{1,0:T(8,128)(2,1)} async-done(((bf16[32,4096]{1,0:T(8,128)(2,1)}), bf16[8,4096]{1,0:T(8,128)(2,1)}) %reduce-scatter.19.cloned.1.call-update) | async-done | bytes 65552
  59.6 0.9 multiply_convert_fusion.1
  60.8 5.7 %fusion.8 = f32[8,32,1,64]{3,2,1,0:T(1,128)S(1)} fusion(f32[8,32,128,1]{2,3,1,0:T(1,128)S(1)} %bitcast.220, f32[2,8,32,64,128]{4,3,2,1,0:T(8,128)} %param.23, f32[8,32,128]{2,1,0:T(8,128)S(1)} %broadcast_bitcast_fusion.1, f32[8,32,64]{2,1,0:T(8,128)S(1)} %broadcast_multiply_fusion.1, f32[8,32]{1,0:T(8,128)S(1)} %get-tuple-element.14), kind=kOutput, calls=%fused_computation.10 | convolution fusion | flops 10485760 | bytes 8782848 | tf_op jit(solution)/shard_map/bhpn,bhn->bhp/dot_general | solution.py:92
  67.3 13.4 %all_gather.13 = bf16[32,2048]{1,0:T(8,128)(2,1)S(1)} all-gather(bf16[8,2048]{1,0:T(8,128)(2,1)S(1)} %fusion.92), channel_id=1, replica_groups=mesh['grp'=2,'tp'=4,'dp'=4] {'dp'}, dimensions={0}, use_global_device_ids=true | all-gather | bytes 163840 | tf_op jit(solution)/shard_map/all_gather | solution.py:101
  80.6 3.7 %fusion.46 = bf16[32,1024]{1,0:T(8,128)(2,1)} fusion(bf16[32,2048]{1,0:T(8,128)(2,1)S(1)} %all_gather.13, bf16[2,2048,1024]{2,1,0:T(8,128)(2,1)} %param.29), kind=kOutput, calls=%fused_computation.41 | convolution fusion | flops 134250496 | bytes 4390912 | tf_op jit(solution)/shard_map/dot_general | solution.py:100
  84.4 17.8 %reduce-scatter.15.cloned.1.call-done = bf16[8,1024]{1,0:T(8,128)(2,1)} async-done(((bf16[32,1024]{1,0:T(8,128)(2,1)}), bf16[8,1024]{1,0:T(8,128)(2,1)}) %reduce-scatter.15.cloned.1.call-update) | async-done | bytes 16400 | tf_op jit(solution)/shard_map/reduce_scatter | solution.py:105
  102.9 5.2 %all_gather.14 = bf16[32,1024]{1,0:T(8,128)(2,1)S(1)} all-gather(bf16[8,1024]{1,0:T(8,128)(2,1)S(1)} %add_convert_fusion.1), channel_id=1, replica_groups=mesh['grp'=2,'tp'=4,'dp'=4] {'tp'}, dimensions={0}, use_global_device_ids=true | all-gather | bytes 81920 | tf_op jit(solution)/shard_map/all_gather | solution.py:35
  108.4 2.1 fusion.58
  110.5 4.9 %fusion.34 = bf16[2,4,8,2048]{3,2,1,0:T(8,128)(2,1)S(1)} fusion(bf16[2,2,1024,2048]{3,2,1,0:T(8,128)(2,1)} %param.16, bf16[32,1024]{1,0:T(8,128)(2,1)S(1)} %all_gather.14, f32[1024]{0:T(1024)S(1)} %bitcast.229), kind=kOutput, calls=%fused_computation.33 | convolution fusion | flops 268664832 | bytes 8720384 | tf_op jit(solution)/shard_map/bd,rdc->brc/dot_general | solution.py:40
  116.1 12.1 %all-reduce.4 = (bf16[32]{0:T(256)(128)(2,1)S(1)}, bf16[32,128]{1,0:T(8,128)(2,1)S(1)}) all-reduce(bf16[32]{0:T(256)(128)(2,1)S(1)} %fusion.71, bf16[32,128]{1,0:T(8,128)(2,1)S(1)} %convolution_convert_fusion), channel_id=8, replica_groups=mesh['grp'=2,'tp'=4,'dp'=4] {'dp'}, use_global_device_ids=true, to_apply=%region_12.13.clone | all-reduce | flops 4128 | bytes 16512
  129.3 6.3 %reduce-scatter.25.cloned.1.call-done = bf16[8,1024]{1,0:T(8,128)(2,1)} async-done(((bf16[32,1024]{1,0:T(8,128)(2,1)}), bf16[8,1024]{1,0:T(8,128)(2,1)}) %reduce-scatter.25.cloned.1.call-update) | async-done | bytes 16400
  137.1 19.3 %reduce-scatter.23.cloned.1.call-done = bf16[8,4096]{1,0:T(8,128)(2,1)} async-done(((bf16[32,4096]{1,0:T(8,128)(2,1)}), bf16[8,4096]{1,0:T(8,128)(2,1)}) %reduce-scatter.23.cloned.1.call-update) | async-done | bytes 65552
  156.4 0.9 multiply_convert_fusion
  157.7 13.0 %multiply_add_fusion.1 = (f32[1,8,32,64,128]{4,3,2,1,0:T(8,128)}, f32[1,8,32,64,128]{4,3,2,1,0:T(8,128)}) fusion(f32[2,8,32,64,128]{4,3,2,1,0:T(8,128)} %param.23, f32[8,32,128]{2,1,0:T(8,128)S(1)} %broadcast_bitcast_fusion.1, f32[8,32,64]{2,1,0:T(8,128)S(1)} %broadcast_multiply_fusion.1, f32[8,32]{1,0:T(8,128)S(1)} %get-tuple-element.14, ...), kind=kLoop, calls=%fused_computation.12 | loop fusion | flops 12582912 | bytes 33949696 | tf_op jit(solution)/shard_map/add | solution.py:89
  170.7 5.7 %fusion.3 = f32[8,32,1,64]{3,2,1,0:T(1,128)S(1)} fusion(f32[8,32,128,1]{2,3,1,0:T(1,128)S(1)} %bitcast.219, f32[2,8,32,64,128]{4,3,2,1,0:T(8,128)} %param.23, f32[8,32,128]{2,1,0:T(8,128)S(1)} %broadcast_bitcast_fusion, f32[8,32,64]{2,1,0:T(8,128)S(1)} %broadcast_multiply_fusion, f32[8,32]{1,0:T(8,128)S(1)} %get-tuple-element.10), kind=kOutput, calls=%fused_computation.5 | convolution fusion | flops 10485760 | bytes 8782848 | tf_op jit(solution)/shard_map/bhpn,bhn->bhp/dot_general | solution.py:92
  177.1 13.3 %all_gather.15 = bf16[32,2048]{1,0:T(8,128)(2,1)S(1)} all-gather(bf16[8,2048]{1,0:T(8,128)(2,1)S(1)} %fusion.93), channel_id=1, replica_groups=mesh['grp'=2,'tp'=4,'dp'=4] {'dp'}, dimensions={0}, use_global_device_ids=true | all-gather | bytes 163840 | tf_op jit(solution)/shard_map/all_gather | solution.py:101
  190.5 3.6 %fusion.49 = bf16[32,1024]{1,0:T(8,128)(2,1)} fusion(bf16[32,2048]{1,0:T(8,128)(2,1)S(1)} %all_gather.15, bf16[2,2048,1024]{2,1,0:T(8,128)(2,1)} %param.29), kind=kOutput, calls=%fused_computation.42 | convolution fusion | flops 134250496 | bytes 4390912 | tf_op jit(solution)/shard_map/dot_general | solution.py:100
  194.2 12.1 %pad_maximum_fusion = f32[2,8,32,64,128]{4,3,2,1,0:T(8,128)} fusion(f32[1,8,32,64,128]{4,3,2,1,0:T(8,128)} %get-tuple-element.17, f32[1,8,32,64,128]{4,3,2,1,0:T(8,128)} %get-tuple-element.16), kind=kLoop, calls=%fused_computation | loop fusion | flops 4194304 | bytes 33554432 | tf_op jit(solution)/shard_map/stack | solution.py:155
  206.9 5.1 %reduce-scatter.17.cloned.1.call-done = bf16[8,1024]{1,0:T(8,128)(2,1)} async-done(((bf16[32,1024]{1,0:T(8,128)(2,1)}), bf16[8,1024]{1,0:T(8,128)(2,1)}) %reduce-scatter.17.cloned.1.call-update) | async-done | bytes 16400 | tf_op jit(solution)/shard_map/reduce_scatter | solution.py:105
  212.1 1.3 add_convert_fusion
  (107 shorter events, 11.8 us)
Async XLA Ops:
  7.2 16.3 %copy-start.10 = (u32[32]{0:T(128)S(1)}, u32[32]{0:T(128)}, u32[]{:S(2)}) copy-start(u32[32]{0:T(128)} %constant.38) | copy-start | bytes 388
  7.2 16.0 %copy-start.6 = (f32[2,32]{1,0:T(2,128)S(1)}, f32[2,32]{1,0:T(2,128)}, u32[]{:S(2)}) copy-start(f32[2,32]{1,0:T(2,128)} %param.26) | copy-start | bytes 772
  7.2 16.0 %copy-start.4 = (bf16[2,2048]{1,0:T(2,128)(2,1)S(1)}, bf16[2,2048]{1,0:T(2,128)(2,1)}, u32[]{:S(2)}) copy-start(bf16[2,2048]{1,0:T(2,128)(2,1)} %param.28) | copy-start | bytes 24580
  7.2 16.1 %copy-start.5 = (bf16[2,2,4,512]{3,2,1,0:T(4,128)(2,1)S(1)}, bf16[2,2,4,512]{3,2,1,0:T(4,128)(2,1)}, u32[]{:S(2)}) copy-start(bf16[2,2,4,512]{3,2,1,0:T(4,128)(2,1)} %param.20) | copy-start | bytes 49156
  7.2 16.1 %copy-start.9 = (bf16[2,1024,128]{2,1,0:T(8,128)(2,1)S(1)}, bf16[2,1024,128]{2,1,0:T(8,128)(2,1)}, u32[]{:S(2)}) copy-start(bf16[2,1024,128]{2,1,0:T(8,128)(2,1)} %param.18) | copy-start | bytes 1572868
  7.2 30.5 %copy-start.3 = (bf16[2,4,2048]{2,1,0:T(4,128)(2,1)S(1)}, bf16[2,4,2048]{2,1,0:T(4,128)(2,1)}, u32[]{:S(2)}) copy-start(bf16[2,4,2048]{2,1,0:T(4,128)(2,1)} %param.19) | copy-start | bytes 98308
  7.2 30.5 %copy-start.1 = (bf16[2,2,8,3,512]{4,2,3,1,0:T(8,128)(2,1)S(1)}, bf16[2,2,8,3,512]{4,2,3,1,0:T(8,128)(2,1)}, u32[]{:S(2)}) copy-start(bf16[2,2,8,3,512]{4,2,3,1,0:T(8,128)(2,1)} %param.22) | copy-start | bytes 294916
  7.2 30.5 %copy-start = (bf16[2,8,3,2048]{3,1,2,0:T(8,128)(2,1)S(1)}, bf16[2,8,3,2048]{3,1,2,0:T(8,128)(2,1)}, u32[]{:S(2)}) copy-start(bf16[2,8,3,2048]{3,1,2,0:T(8,128)(2,1)} %param.21) | copy-start | bytes 589828
  7.3 30.5 %copy-start.7 = (f32[2,32]{1,0:T(2,128)S(1)}, f32[2,32]{1,0:T(2,128)}, u32[]{:S(2)}) copy-start(f32[2,32]{1,0:T(2,128)} %param.25) | copy-start | bytes 772
  7.3 30.5 %copy-start.8 = (f32[2,32]{1,0:T(2,128)S(1)}, f32[2,32]{1,0:T(2,128)}, u32[]{:S(2)}) copy-start(f32[2,32]{1,0:T(2,128)} %param.24) | copy-start | bytes 772
  7.3 31.2 %reduce-scatter.21.cloned.1.call-start = ((), (), s32[]{:S(2)}) async-start(), calls=%async_computation.9 | async-start | bytes 81920
  17.3 42.3 %reduce-scatter.19.cloned.1.call-start = ((), (), s32[]{:S(2)}) async-start(), calls=%async_computation.8 | async-start | bytes 327680
  23.0 79.2 %reduce-scatter.15.cloned.1.call-start = ((), (), s32[]{:S(2)}) async-start(), calls=%async_computation.6 | async-start | bytes 81920 | tf_op jit(solution)/shard_map/reduce_scatter | solution.py:105
  60.8 41.4 %copy-start.2 = (bf16[8,1024]{1,0:T(8,128)(2,1)S(1)}, bf16[8,1024]{1,0:T(8,128)(2,1)}, u32[]{:S(2)}) copy-start(bf16[8,1024]{1,0:T(8,128)(2,1)} %param.15) | copy-start | bytes 49156
  84.3 51.2 %reduce-scatter.25.cloned.1.call-start = ((), (), s32[]{:S(2)}) async-start(), calls=%async_computation.11 | async-start | bytes 81920
  116.1 40.3 %reduce-scatter.23.cloned.1.call-start = ((), (), s32[]{:S(2)}) async-start(), calls=%async_computation.10 | async-start | bytes 327680
  129.1 83.0 %reduce-scatter.17.cloned.1.call-start = ((), (), s32[]{:S(2)}) async-start(), calls=%async_computation.7 | async-start | bytes 81920 | tf_op jit(solution)/shard_map/reduce_scatter | solution.py:105
Sparse Core Ops, SparseCore 0:
  17.4 20.9 reduce-scatter.20
  41.3 18.2 reduce-scatter.18
  84.4 17.7 reduce-scatter.14
  116.2 19.2 reduce-scatter.24
  138.2 18.1 reduce-scatter.22
  194.3 17.7 reduce-scatter.16
where the time goes:
time: 221 us; the launch traced here: 220 us
  waiting for transfers between devices  69.4 us (31%)
  blocking collectives  63.4 us (29%)
  other arithmetic  34.4 us (16%)
  matrix products  33 us (15%)
  between operations  15.2 us (7%)
  local copies, waits for them, and re-layouts  4.53 us (2%)
    unnamed x10, waiting for transfers between devices  46.5 us
    all_gather x2, blocking collectives, mixer_step(): lax.all_gather(normed, 'dp', axis=0, tiled=True)  26.7 us
    unnamed x2, blocking collectives  25 us
    reduce_scatter x2, waiting for transfers between devices, mixer_step(): lax.psum_scatter(out_terms.astype(jnp.bfloat16), 'tp', scatter_dimension=...  23 us
    another operation x7, other arithmetic, shards(): return (current, jnp.stack(convs), jnp.stack(vec_rows), jnp.stack(states))  13.5 us
    add x1, other arithmetic, mixer_step(): decay[:, :, None, None] * ssm_state[layer]  13 us
    all_gather x2, blocking collectives, mixer_step(): whole_rows = lax.all_gather(current, 'tp', axis=0, tiled=True)  11.7 us
    dot_general x2, matrix products, mixer_step(): jnp.einsum('bhpn,bhn->bhp', state, out_vec)  11.5 us
  transfers between devices with their start and end apart: 6, of which 6 were waited for; matrix products, arithmetic and copies ran while one was open for 10% of the time, Pallas kernels for 0%

commit v1 on v0

v1 whole, which is shorter than its diff:
```python
import functools

import jax
import jax.numpy as jnp
from jax import lax
from jax.experimental import pallas as pl
from jax.experimental.pallas import tpu as pltpu
from jax.sharding import PartitionSpec as P

MODEL_WIDTH = 4096
HEAD_COUNT = 128
HEAD_DIM = 64
STATE_DIM = 128
GROUP_COUNT = 16
LAYER_COUNT = 2

EPS = 1e-06
F32 = jnp.float32
BF16 = jnp.bfloat16


def remote(src, dst, send_sem, recv_sem, axis, target):
    return pltpu.make_async_remote_copy(
        src_ref=src,
        dst_ref=dst,
        send_sem=send_sem,
        recv_sem=recv_sem,
        device_id={axis: target},
        device_id_type=pl.DeviceIdType.MESH,
    )


def greet(sizes):
    barrier = pltpu.get_barrier_semaphore()
    count = 0
    for axis, n in sizes:
        me = lax.axis_index(axis)
        for k in range(1, n):
            pl.semaphore_signal(
                barrier,
                inc=1,
                device_id={axis: lax.rem(me + k, n)},
                device_id_type=pl.DeviceIdType.MESH,
            )
            count += 1
    pl.semaphore_wait(barrier, count)


def spread(src, dst, send_sem, recv_sem, axis, n):
    me = lax.axis_index(axis)
    copies = []
    for k in range(1, n):
        copy = remote(src, dst.at[me], send_sem.at[k], recv_sem.at[k], axis, lax.rem(me + k, n))
        copy.start()
        copies.append(copy)
    return copies


def deal(src, dst, send_sem, recv_sem, axis, n, whole=False):
    me = lax.axis_index(axis)
    copies = []
    for k in range(1, n):
        peer = lax.rem(me + k, n)
        copy = remote(
            src if whole else src.at[peer],
            dst.at[k],
            send_sem.at[k],
            recv_sem.at[k],
            axis,
            peer,
        )
        copy.start()
        copies.append(copy)
    return copies


def project(
    layer, ndp, rows_d, lhs, squares, weights, loads, w_step_ref, send, recv, sems, outs
):
    w_in_buf, w_vec_buf = weights
    load_in, load_vec = loads
    send_gate, send_val, send_small = send
    recv_gate, recv_val, recv_small = recv
    proj_ref, vecs_ref, step_ref = outs
    vec_cols = w_vec_buf.shape[2]
    cols = w_in_buf.shape[2]
    heads = w_step_ref.shape[2]
    me = lax.axis_index("dp")

    def put(target, at, acc):
        for p in range(ndp):
            target[p, :, at : at + acc.shape[1]] = acc[p * rows_d : (p + 1) * rows_d].astype(BF16)

    put(send_small, 2 * vec_cols, jnp.dot(lhs, w_step_ref[layer], preferred_element_type=F32))
    put(send_small, 2 * vec_cols + heads, jnp.broadcast_to(squares, (squares.shape[0], 128)))
    load_vec.wait()
    for role in range(2):
        put(send_small, role * vec_cols, jnp.dot(lhs, w_vec_buf[role], preferred_element_type=F32))
    copies = deal(send_small, recv_small, sems[0], sems[1], "dp", ndp)
    block = min(cols, 1024)
    for role in (0, 1):
        target, landing = ((send_gate, recv_gate), (send_val, recv_val))[role]
        load_in[role].wait()
        for at in range(0, cols, block):
            put(
                target,
                at,
                jnp.dot(lhs, w_in_buf[role, :, at : at + block], preferred_element_type=F32),
            )
        copies += deal(target, landing, sems[2 + 2 * role], sems[3 + 2 * role], "dp", ndp)
    for copy in copies:
        copy.wait()

    def total(mine, others):
        acc = mine[me].astype(F32)
        for k in range(1, ndp):
            acc = acc + others[k].astype(F32)
        return acc

    small = total(send_small, recv_small)
    own_sq = small[:, 2 * vec_cols + heads : 2 * vec_cols + heads + 1]
    scale = lax.rsqrt(own_sq * (1.0 / MODEL_WIDTH) + EPS)
    for role in range(2):
        vecs_ref[role] = (small[:, role * vec_cols : (role + 1) * vec_cols] * scale).astype(BF16)
    step_ref[...] = small[:, 2 * vec_cols : 2 * vec_cols + heads] * scale
    proj_ref[0] = (total(send_gate, recv_gate) * scale).astype(BF16)
    proj_ref[1] = (total(send_val, recv_val) * scale).astype(BF16)


def first_kernel(
    ntp, ndp, x_ref, gain_ref, w_step_ref, w_in_ref, w_vec_ref,
    proj_ref, vecs_ref, step_ref, all_ref,
    w_in_buf, w_vec_buf, lhs_buf, landed, send_gate, send_val, send_small,
    recv_gate, recv_val, recv_small, load_sem, ssem_x, rsem_x, *sems,
):
    rows_t = x_ref.shape[0]
    load_vec = pltpu.make_async_copy(w_vec_ref.at[0], w_vec_buf, load_sem.at[0])
    load_vec.start()
    load_in = []
    for role in range(2):
        copy = pltpu.make_async_copy(w_in_ref.at[0, role], w_in_buf.at[role], load_sem.at[1 + role])
        copy.start()
        load_in.append(copy)
    greet((("tp", ntp), ("dp", ndp)))
    copies = spread(x_ref, landed, ssem_x, rsem_x, "tp", ntp)
    landed[lax.axis_index("tp")] = x_ref[...]
    gain = gain_ref[...].astype(F32)[0:1]
    for copy in copies:
        copy.wait()
    squares = []
    for i in range(ntp):
        part = landed[i]
        all_ref[i] = part
        part = part.astype(F32)
        squares.append(jnp.sum(part * part, axis=1, keepdims=True))
        lhs_buf[i * rows_t : (i + 1) * rows_t, :] = part * gain
    squares = jnp.concatenate(squares, axis=0)
    project(
        0, ndp, proj_ref.shape[1], lhs_buf[...].astype(BF16), squares, (w_in_buf, w_vec_buf),
        (load_in, load_vec), w_step_ref, (send_gate, send_val, send_small),
        (recv_gate, recv_val, recv_small), sems, (proj_ref, vecs_ref, step_ref),
    )


def gather_normed(ndp, normed_ref, held, lhs_out, send_sem, recv_sem):
    rows_d = normed_ref.shape[0]
    copies = spread(normed_ref, held, send_sem, recv_sem, "dp", ndp)
    held[lax.axis_index("dp")] = normed_ref[...]
    for copy in copies:
        copy.wait()
    for i in range(ndp):
        lhs_out[i * rows_d : (i + 1) * rows_d, :] = held[i].astype(F32)
    return lhs_out[...].astype(BF16)


def middle_kernel(
    layer, ntp, ndp, normed_ref, old_ref, gain_ref, w_step_ref, w_out_ref, w_in_ref, w_vec_ref,
    proj_ref, vecs_ref, step_ref, all_ref,
    w_out_buf, w_in_buf, w_vec_buf, lhs_out, lhs_buf, held, part_out, parts_in,
    send_gate, send_val, send_small, recv_gate, recv_val, recv_small,
    load_sem, ssem_n, rsem_n, ssem_o, rsem_o, *sems,
):
    rows_t = old_ref.shape[1]
    load_out = pltpu.make_async_copy(w_out_ref.at[layer - 1], w_out_buf, load_sem.at[3])
    load_out.start()
    load_vec = pltpu.make_async_copy(w_vec_ref.at[layer], w_vec_buf, load_sem.at[0])
    load_vec.start()
    load_in = []
    for role in range(2):
        copy = pltpu.make_async_copy(
            w_in_ref.at[layer, role], w_in_buf.at[role], load_sem.at[1 + role]
        )
        copy.start()
        load_in.append(copy)
    greet((("tp", ntp), ("dp", ndp)))
    lhs = gather_normed(ndp, normed_ref, held, lhs_out, ssem_n, rsem_n)
    gain = gain_ref[...].astype(F32)[layer : layer + 1]
    load_out.wait()
    part_out[...] = jnp.dot(lhs, w_out_buf[...], preferred_element_type=F32).astype(BF16)
    copies = deal(part_out, parts_in, ssem_o, rsem_o, "tp", ntp, whole=True)
    for copy in copies:
        copy.wait()
    acc = part_out[...].astype(F32)
    for k in range(1, ntp):
        acc = acc + parts_in[k].astype(F32)
    squares = []
    for i in range(ntp):
        part = (old_ref[i].astype(F32) + acc[i * rows_t : (i + 1) * rows_t]).astype(BF16)
        all_ref[i] = part
        part = part.astype(F32)
        squares.append(jnp.sum(part * part, axis=1, keepdims=True))
        lhs_buf[i * rows_t : (i + 1) * rows_t, :] = part * gain
    squares = jnp.concatenate(squares, axis=0)
    project(
        layer, ndp, proj_ref.shape[1], lhs_buf[...].astype(BF16), squares, (w_in_buf, w_vec_buf),
        (load_in, load_vec), w_step_ref, (send_gate, send_val, send_small),
        (recv_gate, recv_val, recv_small), sems, (proj_ref, vecs_ref, step_ref),
    )


def last_kernel(
    layer, ntp, ndp, normed_ref, old_ref, w_out_ref, out_ref,
    w_out_buf, lhs_out, held, send_out, recv_out, load_sem, ssem_n, rsem_n, ssem_o, rsem_o,
):
    rows_t = old_ref.shape[1]
    load_out = pltpu.make_async_copy(w_out_ref.at[layer], w_out_buf, load_sem)
    load_out.start()
    greet((("tp", ntp), ("dp", ndp)))
    lhs = gather_normed(ndp, normed_ref, held, lhs_out, ssem_n, rsem_n)
    load_out.wait()
    acc = jnp.dot(lhs, w_out_buf[...], preferred_element_type=F32)
    for i in range(ntp):
        send_out[i] = acc[i * rows_t : (i + 1) * rows_t].astype(BF16)
    me = lax.axis_index("tp")
    copies = deal(send_out, recv_out, ssem_o, rsem_o, "tp", ntp)
    for copy in copies:
        copy.wait()
    acc = send_out[me].astype(F32)
    for k in range(1, ntp):
        acc = acc + recv_out[k].astype(F32)
    out_ref[...] = (old_ref[me].astype(F32) + acc).astype(BF16)


VMEM = pl.BlockSpec(memory_space=pltpu.VMEM)
HBM = pl.BlockSpec(memory_space=pl.ANY)


def sizes_of(tokens, w_in, w_vec, w_step, ntp, ndp):
    rows_t, width = tokens.shape
    batch = rows_t * ntp
    return rows_t, width, batch, batch // ndp, w_in.shape[3], w_vec.shape[3], w_step.shape[2]


def dma(n):
    return pltpu.SemaphoreType.DMA((n,))


def mixer_scratch(width, cols, vcols, heads, rows_d, ndp):
    small = 2 * vcols + heads + 128
    return [
        pltpu.VMEM((2, width, cols), BF16),
        pltpu.VMEM((2, width, vcols), BF16),
    ], [
        pltpu.VMEM((ndp, rows_d, cols), BF16),
        pltpu.VMEM((ndp, rows_d, cols), BF16),
        pltpu.VMEM((ndp, rows_d, small), BF16),
        pltpu.VMEM((ndp, rows_d, cols), BF16),
        pltpu.VMEM((ndp, rows_d, cols), BF16),
        pltpu.VMEM((ndp, rows_d, small), BF16),
    ]


def first_call(ntp, ndp, tokens, mix_gain, w_step, w_in, w_vec):
    rows_t, width, batch, rows_d, cols, vcols, heads = sizes_of(
        tokens, w_in, w_vec, w_step, ntp, ndp
    )
    bufs, wires = mixer_scratch(width, cols, vcols, heads, rows_d, ndp)
    return pl.pallas_call(
        functools.partial(first_kernel, ntp, ndp),
        out_shape=(
            jax.ShapeDtypeStruct((2, rows_d, cols), BF16),
            jax.ShapeDtypeStruct((2, rows_d, vcols), BF16),
            jax.ShapeDtypeStruct((rows_d, heads), F32),
            jax.ShapeDtypeStruct((ntp, rows_t, width), BF16),
        ),
        in_specs=[VMEM, VMEM, VMEM, HBM, HBM],
        out_specs=(VMEM,) * 4,
        scratch_shapes=bufs
        + [pltpu.VMEM((batch, width), F32), pltpu.VMEM((ntp, rows_t, width), BF16)]
        + wires
        + [dma(3), dma(ntp), dma(ntp)]
        + [dma(ndp)] * 6,
        compiler_params=pltpu.CompilerParams(collective_id=0, has_side_effects=True),
    )(tokens, mix_gain, w_step, w_in, w_vec)


def middle_call(layer, ntp, ndp, tokens, normed, old, mix_gain, w_step, w_out, w_in, w_vec):
    rows_t, width, batch, rows_d, cols, vcols, heads = sizes_of(
        tokens, w_in, w_vec, w_step, ntp, ndp
    )
    bufs, wires = mixer_scratch(width, cols, vcols, heads, rows_d, ndp)
    return pl.pallas_call(
        functools.partial(middle_kernel, layer, ntp, ndp),
        out_shape=(
            jax.ShapeDtypeStruct((2, rows_d, cols), BF16),
            jax.ShapeDtypeStruct((2, rows_d, vcols), BF16),
            jax.ShapeDtypeStruct((rows_d, heads), F32),
            jax.ShapeDtypeStruct((ntp, rows_t, width), BF16),
        ),
        in_specs=[VMEM, VMEM, VMEM, VMEM, HBM, HBM, HBM],
        out_specs=(VMEM,) * 4,
        scratch_shapes=[pltpu.VMEM((cols, width), BF16)]
        + bufs
        + [
            pltpu.VMEM((batch, cols), F32),
            pltpu.VMEM((batch, width), F32),
            pltpu.VMEM((ndp, rows_d, cols), BF16),
            pltpu.VMEM((batch, width), BF16),
            pltpu.VMEM((ntp, batch, width), BF16),
        ]
        + wires
        + [dma(4), dma(ndp), dma(ndp), dma(ntp), dma(ntp)]
        + [dma(ndp)] * 6,
        compiler_params=pltpu.CompilerParams(collective_id=layer, has_side_effects=True),
    )(normed, old, mix_gain, w_step, w_out, w_in, w_vec)


def last_call(layer, ntp, ndp, normed, old, w_out):
    _, rows_t, width = old.shape
    rows_d, cols = normed.shape
    batch = rows_t * ntp
    return pl.pallas_call(
        functools.partial(last_kernel, layer, ntp, ndp),
        out_shape=jax.ShapeDtypeStruct((rows_t, width), BF16),
        in_specs=[VMEM, VMEM, HBM],
        out_specs=VMEM,
        scratch_shapes=[
            pltpu.VMEM((cols, width), BF16),
            pltpu.VMEM((batch, cols), F32),
            pltpu.VMEM((ndp, rows_d, cols), BF16),
            pltpu.VMEM((ntp, rows_t, width), BF16),
            pltpu.VMEM((ntp, rows_t, width), BF16),
            pltpu.SemaphoreType.DMA,
            dma(ndp), dma(ndp), dma(ntp), dma(ntp),
        ],
        compiler_params=pltpu.CompilerParams(collective_id=layer + 1, has_side_effects=True),
    )(normed, old, w_out)


def head_step(
    layer, proj, vecs, step_all, conv_weight, conv_vec, conv_state, vec_state, ssm_state,
    step_bias, decay_log, skip_gain, out_gain,
):
    local_rows, columns = proj.shape[1:]
    vec_columns = vecs.shape[2]
    local_heads = ssm_state.shape[2]
    head_start = lax.axis_index("tp") * local_heads
    step_raw = lax.dynamic_slice_in_dim(step_all, head_start, local_heads, 1)
    window = jnp.concatenate([conv_state[layer], proj[1][:, None, :]], axis=1)
    new_conv = window[:, 1:, :]
    values_sum = jnp.sum(
        window.astype(jnp.float32) * conv_weight[layer].astype(jnp.float32)[None, :, :], axis=1
    )
    fresh = vecs[:, :, None, :]
    vec_window = jnp.concatenate([vec_state[layer], fresh], axis=2)
    new_vec = vec_window[:, :, 1:, :]
    vec_sum = jnp.sum(
        vec_window.astype(jnp.float32) * conv_vec[layer].astype(jnp.float32)[:, None, :, :], axis=2
    )
    values = jax.nn.silu(values_sum).reshape(local_rows, local_heads, HEAD_DIM)
    vec_act = jax.nn.silu(vec_sum)
    local_groups = vec_columns // STATE_DIM
    repeat = HEAD_COUNT // GROUP_COUNT
    in_vec = jnp.repeat(vec_act[0].reshape(local_rows, local_groups, STATE_DIM), repeat, axis=1)
    out_vec = jnp.repeat(vec_act[1].reshape(local_rows, local_groups, STATE_DIM), repeat, axis=1)
    step = jax.nn.softplus(step_raw + step_bias[layer][None, :])
    decay = jnp.exp(-step * jnp.exp(decay_log[layer])[None, :])
    state = (
        decay[:, :, None, None] * ssm_state[layer]
        + (step[:, :, None] * values)[..., None] * in_vec[:, :, None, :]
    )
    read = jnp.einsum("bhpn,bhn->bhp", state, out_vec) + skip_gain[layer][None, :, None] * values
    mixed = read.reshape(local_rows, columns) * jax.nn.silu(proj[0].astype(jnp.float32))
    grouped = mixed.reshape(local_rows, local_groups, columns // local_groups)
    grouped = grouped * lax.rsqrt(jnp.mean(grouped * grouped, axis=2, keepdims=True) + EPS)
    normed = (grouped.reshape(local_rows, columns) * out_gain[layer].astype(jnp.float32)).astype(
        jnp.bfloat16
    )
    return (normed, new_conv, new_vec, state)


def shards(
    ntp,
    ndp,
    tokens,
    w_in,
    w_vec,
    w_step,
    conv_weight,
    conv_vec,
    conv_state,
    vec_state,
    ssm_state,
    step_bias,
    decay_log,
    skip_gain,
    mix_gain,
    out_gain,
    w_out,
):
    convs = []
    vec_rows = []
    states = []
    for layer in range(LAYER_COUNT):
        if layer == 0:
            proj, vecs, step_all, rows = first_call(
                ntp, ndp, tokens, mix_gain, w_step, w_in, w_vec
            )
        else:
            proj, vecs, step_all, rows = middle_call(
                layer, ntp, ndp, tokens, normed, rows, mix_gain, w_step, w_out, w_in, w_vec
            )
        normed, conv_next, vec_next, state_next = head_step(
            layer, proj, vecs, step_all, conv_weight, conv_vec, conv_state, vec_state,
            ssm_state, step_bias, decay_log, skip_gain, out_gain,
        )
        convs.append(conv_next)
        vec_rows.append(vec_next)
        states.append(state_next)
    current = last_call(LAYER_COUNT - 1, ntp, ndp, normed, rows, w_out)
    return (current, jnp.stack(convs), jnp.stack(vec_rows), jnp.stack(states))


def solution(mesh):
    placed = (
        P(("grp", "tp"), "dp"),
        P(None, None, "dp", "tp"),
        P(None, None, "dp", "tp"),
        P(None, "dp", None),
        P(None, None, "tp"),
        P(None, None, None, "tp"),
        P(None, ("grp", "dp"), None, "tp"),
        P(None, None, ("grp", "dp"), None, "tp"),
        P(None, ("grp", "dp"), "tp", None, None),
        P(None, "tp"),
        P(None, "tp"),
        P(None, "tp"),
        P(None, "dp"),
        P(None, "tp"),
        P(None, "tp", "dp"),
    )
    return jax.shard_map(
        functools.partial(shards, mesh.shape["tp"], mesh.shape["dp"]),
        mesh=mesh,
        in_specs=placed,
        out_specs=(
            P(("grp", "tp"), "dp"),
            P(None, ("grp", "dp"), None, "tp"),
            P(None, None, ("grp", "dp"), None, "tp"),
            P(None, ("grp", "dp"), "tp", None, None),
        ),
        check_vma=False,
    )
```

time: 221 us -> 97.6 us (0.44)
  waiting for transfers between devices: 69.4 us -> 0 us
  blocking collectives: 63.4 us -> 0 us
  Pallas kernels: 0 us -> 53.8 us
  matrix products: 33 us -> 11.4 us
  between operations: 15.2 us -> 0.88 us
  other arithmetic: 34.4 us -> 25.6 us
    pallas_call x0 -> x3, Pallas kernels: none -> 53.8 us  [the longest x1 23.2 us: middle_call(): pl.pallas_call(functools.partial(middle_kernel, layer, ntp, ndp), out_sha...]
    unnamed x10 -> x0, waiting for transfers between devices: 46.5 us -> none
    all_gather x4 -> x0, blocking collectives: 38.4 us -> none  [the longest x2 26.7 us: mixer_step(): lax.all_gather(normed, 'dp', axis=0, tiled=True)]
    unnamed x2 -> x0, blocking collectives: 25 us -> none
    reduce_scatter x2 -> x0, waiting for transfers between devices: 23 us -> none  [mixer_step(): lax.psum_scatter(out_terms.astype(jnp.bfloat16), 'tp', scatter_dimension=...]
    dot_general x10 -> x2, matrix products: 33 us -> 11.4 us  [head_step(): jnp.einsum('bhpn,bhn->bhp', state, out_vec)]
    another operation x7 -> x5, other arithmetic: 13.5 us -> 8.34 us  [shards(): return (current, jnp.stack(convs), jnp.stack(vec_rows), jnp.stack(states))]
    add x1, other arithmetic: 13 us -> 8.13 us  [head_step(): decay[:, :, None, None] * ssm_state[layer]]
  transfers between devices with their start and end apart: 6 -> 0, of which waited for: 6 -> 0; matrix products, arithmetic and copies ran while one was open for 10% -> 0% of each run, Pallas kernels for 0% -> 0%
where the time goes in v1:
time: 97.6 us; the launch traced here: 96.6 us
  Pallas kernels  53.8 us (55%)
  other arithmetic  25.6 us (26%)
  matrix products  11.4 us (12%)
  local copies, waits for them, and re-layouts  4.85 us (5%)
    pallas_call x1, Pallas kernels, middle_call(): pl.pallas_call(functools.partial(middle_kernel, layer, ntp, ndp), out_sha...  23.2 us
    pallas_call x1, Pallas kernels, first_call(): pl.pallas_call(functools.partial(first_kernel, ntp, ndp), out_shape=(jax....  19.5 us
    dot_general x2, matrix products, head_step(): jnp.einsum('bhpn,bhn->bhp', state, out_vec)  11.4 us
    pallas_call x1, Pallas kernels, last_call(): pl.pallas_call(functools.partial(last_kernel, layer, ntp, ndp), out_shape...  11.2 us
    another operation x5, other arithmetic, shards(): return (current, jnp.stack(convs), jnp.stack(vec_rows), jnp.stack(states))  8.34 us
    add x1, other arithmetic, head_step(): decay[:, :, None, None] * ssm_state[layer]  8.13 us

profile of v1, /device:TPU:0, one launch (start us, length us, event | category | flops | bytes accessed | tf_op | source)
XLA Modules:
  0.0 96.6 jit_solution(3321438762363078795)
XLA Ops:
  0.6 0.8 slice_bitcast_fusion.9
  1.4 0.8 exponential_bitcast_fusion
  2.2 0.8 slice_bitcast_fusion.8
  2.9 0.8 slice_convert_fusion.2
  3.7 0.7 bitcast_convert_fusion.2
  4.4 0.7 bitcast_convert_fusion
  5.2 0.8 slice_bitcast_fusion.2
  6.0 19.5 %shard_map.174 = (bf16[2,8,2048]{2,1,0:T(8,128)(2,1)}, bf16[2,8,512]{2,1,0:T(8,128)(2,1)}, f32[8,128]{1,0:T(8,128)}, bf16[4,8,1024]{2,1,0:T(8,128)(2,1)}) custom-call(bf16[8,1024]{1,0:T(8,128)(2,1)} %x_ref.1, bf16[2,1024]{1,0:T(2,128)(2,1)} %gain_ref.3, bf16[2,1024,128]{2,1,0:T(8,128)(2,1)} %w_step_ref.3, bf16[2,2,1024,2048]{3,2,1,0:T(8,128)(2,1)} %w_in_ref.3, ...), custom_call_target="tpu_custom_call" | custom-call | tf_op jit(solution)/shard_map/pallas_call | solution.py:278
  25.5 0.8 multiply_exponential_fusion.1
  26.3 0.7 multiply_reduce_fusion.5
  27.1 0.8 slice_bitcast_fusion.5
  28.3 5.7 %fusion.4 = f32[8,32,1,64]{3,2,1,0:T(1,128)S(1)} fusion(f32[8,32,128,1]{2,3,1,0:T(1,128)S(1)} %bitcast.130, f32[2,8,32,64,128]{4,3,2,1,0:T(8,128)} %param.23, f32[8,32,128]{2,1,0:T(8,128)S(1)} %broadcast_bitcast_fusion.1, f32[8,32,64]{2,1,0:T(8,128)S(1)} %broadcast_multiply_fusion.1, f32[8,32]{1,0:T(8,128)S(1)} %get-tuple-element.26), kind=kOutput, calls=%fused_computation.6 | convolution fusion | flops 10485760 | bytes 8782848 | tf_op jit(solution)/shard_map/bhpn,bhn->bhp/dot_general | solution.py:382
  34.6 0.7 fusion.32.normed_ref
  35.3 23.2 %shard_map.175 = (bf16[2,8,2048]{2,1,0:T(8,128)(2,1)}, bf16[2,8,512]{2,1,0:T(8,128)(2,1)}, f32[8,128]{1,0:T(8,128)}, bf16[4,8,1024]{2,1,0:T(8,128)(2,1)}) custom-call(bf16[8,2048]{1,0:T(8,128)(2,1)} %fusion.32.normed_ref, bf16[4,8,1024]{2,1,0:T(8,128)(2,1)} %get-tuple-element.15.old_ref, bf16[2,1024]{1,0:T(2,128)(2,1)} %gain_ref.3, ...), custom_call_target="tpu_custom_call" | custom-call | tf_op jit(solution)/shard_map/pallas_call | solution.py:302
  58.5 0.8 multiply_exponential_fusion
  59.3 0.7 multiply_reduce_fusion.3
  60.1 0.7 fusion.35
  61.5 0.8 slice_bitcast_fusion.4
  62.4 0.7 pad_maximum_fusion.1
  63.4 5.7 %fusion.1 = f32[8,32,1,64]{3,2,1,0:T(1,128)S(1)} fusion(f32[8,32,128,1]{2,3,1,0:T(1,128)S(1)} %bitcast.131, f32[2,8,32,64,128]{4,3,2,1,0:T(8,128)} %param.23, f32[8,32,128]{2,1,0:T(8,128)S(1)} %broadcast_bitcast_fusion, f32[8,32,64]{2,1,0:T(8,128)S(1)} %broadcast_multiply_fusion, f32[8,32]{1,0:T(8,128)S(1)} %get-tuple-element.22), kind=kOutput, calls=%fused_computation.3 | convolution fusion | flops 10485760 | bytes 8782848 | tf_op jit(solution)/shard_map/bhpn,bhn->bhp/dot_general | solution.py:382
  69.7 0.7 fusion.33.normed_ref
  70.4 11.2 %shard_map.176 = bf16[8,1024]{1,0:T(8,128)(2,1)} custom-call(bf16[8,2048]{1,0:T(8,128)(2,1)} %fusion.33.normed_ref, bf16[4,8,1024]{2,1,0:T(8,128)(2,1)} %get-tuple-element.19.old_ref, bf16[2,2048,1024]{2,1,0:T(8,128)(2,1)} %w_out_ref.3), custom_call_target="tpu_custom_call" | custom-call | tf_op jit(solution)/shard_map/pallas_call | solution.py:332
  81.6 8.1 %multiply_add_fusion.1 = (f32[1,8,32,64,128]{4,3,2,1,0:T(8,128)S(1)}, f32[1,8,32,64,128]{4,3,2,1,0:T(8,128)S(1)}) fusion(f32[2,8,32,64,128]{4,3,2,1,0:T(8,128)} %param.23, f32[8,32,128]{2,1,0:T(8,128)S(1)} %broadcast_bitcast_fusion.1, f32[8,32,64]{2,1,0:T(8,128)S(1)} %broadcast_multiply_fusion.1, f32[8,32]{1,0:T(8,128)S(1)} %get-tuple-element.26, ...), kind=kLoop, calls=%fused_computation.8 | loop fusion | flops 12582912 | bytes 33949696 | tf_op jit(solution)/shard_map/add | solution.py:379
  89.7 6.2 %pad_maximum_fusion = f32[2,8,32,64,128]{4,3,2,1,0:T(8,128)} fusion(f32[1,8,32,64,128]{4,3,2,1,0:T(8,128)S(1)} %get-tuple-element.29, f32[1,8,32,64,128]{4,3,2,1,0:T(8,128)S(1)} %get-tuple-element.28), kind=kLoop, calls=%fused_computation | loop fusion | flops 4194304 | bytes 33554432 | tf_op jit(solution)/shard_map/stack | solution.py:431
  (48 shorter events, 3.3 us)
Async XLA Ops:
  6.0 22.0 %copy-start = (bf16[2,8,3,2048]{3,1,2,0:T(8,128)(2,1)S(1)}, bf16[2,8,3,2048]{3,1,2,0:T(8,128)(2,1)}, u32[]{:S(2)}) copy-start(bf16[2,8,3,2048]{3,1,2,0:T(8,128)(2,1)} %param.21) | copy-start | bytes 589828
  25.5 9.2 %copy-start.2 = (bf16[2,8,2048]{2,1,0:T(8,128)(2,1)S(1)}, bf16[2,8,2048]{2,1,0:T(8,128)(2,1)}, u32[]{:S(2)}) copy-start(bf16[2,8,2048]{2,1,0:T(8,128)(2,1)} %get-tuple-element.13) | copy-start | bytes 196612
  35.3 24.8 %copy-start.4 = (bf16[2,8,512]{2,1,0:T(8,128)(2,1)S(1)}, bf16[2,8,512]{2,1,0:T(8,128)(2,1)}, u32[]{:S(2)}) copy-start(bf16[2,8,512]{2,1,0:T(8,128)(2,1)} %get-tuple-element.14) | copy-start | bytes 49156
  58.5 11.2 %copy-start.1 = (bf16[2,8,2048]{2,1,0:T(8,128)(2,1)S(1)}, bf16[2,8,2048]{2,1,0:T(8,128)(2,1)}, u32[]{:S(2)}) copy-start(bf16[2,8,2048]{2,1,0:T(8,128)(2,1)} %get-tuple-element.17) | copy-start | bytes 196612
  89.7 6.3 %copy-start.3 = (bf16[8,1024]{1,0:T(8,128)(2,1)S(1)}, bf16[8,1024]{1,0:T(8,128)(2,1)}, u32[]{:S(2)}) copy-start(bf16[8,1024]{1,0:T(8,128)(2,1)} %shard_map.176) | copy-start | bytes 49156

commit v2 on v1

--- a/solution.py
+++ b/solution.py
@@ -386,7 +386,7 @@
     normed = (grouped.reshape(local_rows, columns) * out_gain[layer].astype(jnp.float32)).astype(
         jnp.bfloat16
     )
-    return (normed, new_conv, new_vec, state)
+    return (normed, new_conv, new_vec, (decay, step[:, :, None] * values, in_vec))
 
 
 def shards(
@@ -428,7 +428,11 @@
         vec_rows.append(vec_next)
         states.append(state_next)
     current = last_call(LAYER_COUNT - 1, ntp, ndp, normed, rows, w_out)
-    return (current, jnp.stack(convs), jnp.stack(vec_rows), jnp.stack(states))
+    decays, drives, inputs = (jnp.stack(parts) for parts in zip(*states))
+    new_ssm = (
+        decays[..., None, None] * ssm_state + drives[..., None] * inputs[:, :, :, None, :]
+    )
+    return (current, jnp.stack(convs), jnp.stack(vec_rows), new_ssm)
 
 
 def solution(mesh):

time: 97.6 us -> 96.6 us (0.990)
  other arithmetic: 25.6 us -> 24.4 us
    another operation x5 -> x7, other arithmetic: 8.34 us -> 2.16 us  [the longest x4 2.1 us: shards(): return (current, jnp.stack(convs), jnp.stack(vec_rows), new_ssm)]
    add x1, other arithmetic: 8.13 us -> 13 us  [shards(): decays[..., None, None] * ssm_state]
where the time goes in v2:
time: 96.6 us; the launch traced here: 95.6 us
  Pallas kernels  53.8 us (56%)
  other arithmetic  24.4 us (25%)
  matrix products  11.4 us (12%)
  local copies, waits for them, and re-layouts  5.04 us (5%)
    pallas_call x1, Pallas kernels, middle_call(): pl.pallas_call(functools.partial(middle_kernel, layer, ntp, ndp), out_sha...  23.2 us
    pallas_call x1, Pallas kernels, first_call(): pl.pallas_call(functools.partial(first_kernel, ntp, ndp), out_shape=(jax....  19.5 us
    add x1, other arithmetic, shards(): decays[..., None, None] * ssm_state  13 us
    dot_general x2, matrix products, head_step(): jnp.einsum('bhpn,bhn->bhp', state, out_vec)  11.4 us
    pallas_call x1, Pallas kernels, last_call(): pl.pallas_call(functools.partial(last_kernel, layer, ntp, ndp), out_shape...  11.2 us
    another operation x4, other arithmetic, shards(): return (current, jnp.stack(convs), jnp.stack(vec_rows), new_ssm)  2.1 us

profile of v2, /device:TPU:0, one launch (start us, length us, event | category | flops | bytes accessed | tf_op | source)
XLA Modules:
  0.0 95.6 jit_solution(13292287167607434752)
XLA Ops:
  0.6 0.8 slice_bitcast_fusion.9
  1.4 0.8 exponential_bitcast_fusion
  2.2 0.8 slice_bitcast_fusion.8
  2.9 0.8 slice_convert_fusion.2
  3.7 0.7 bitcast_convert_fusion.2
  4.4 0.7 bitcast_convert_fusion
  5.2 0.8 slice_bitcast_fusion.2
  6.0 19.5 %shard_map.174 = (bf16[2,8,2048]{2,1,0:T(8,128)(2,1)}, bf16[2,8,512]{2,1,0:T(8,128)(2,1)}, f32[8,128]{1,0:T(8,128)}, bf16[4,8,1024]{2,1,0:T(8,128)(2,1)}) custom-call(bf16[8,1024]{1,0:T(8,128)(2,1)} %x_ref.1, bf16[2,1024]{1,0:T(2,128)(2,1)} %gain_ref.3, bf16[2,1024,128]{2,1,0:T(8,128)(2,1)} %w_step_ref.3, bf16[2,2,1024,2048]{3,2,1,0:T(8,128)(2,1)} %w_in_ref.3, ...), custom_call_target="tpu_custom_call" | custom-call | tf_op jit(solution)/shard_map/pallas_call | solution.py:278
  25.5 0.8 multiply_exponential_fusion.1
  26.3 0.7 multiply_reduce_fusion.5
  27.1 0.8 slice_bitcast_fusion.5
  28.4 5.7 %fusion.4 = f32[8,32,1,64]{3,2,1,0:T(1,128)S(1)} fusion(f32[8,32,128,1]{2,3,1,0:T(1,128)S(1)} %bitcast.137, f32[2,8,32,64,128]{4,3,2,1,0:T(8,128)} %param.23, f32[8,32,128]{2,1,0:T(8,128)S(1)} %get-tuple-element.43, f32[8,32,64]{2,1,0:T(8,128)S(1)} %broadcast_multiply_fusion.1, f32[8,32]{1,0:T(8,128)S(1)} %get-tuple-element.26), kind=kOutput, calls=%fused_computation.6 | convolution fusion | flops 10485760 | bytes 8782848 | tf_op jit(solution)/shard_map/bhpn,bhn->bhp/dot_general | solution.py:382
  34.7 0.7 fusion.32.normed_ref
  35.4 23.2 %shard_map.175 = (bf16[2,8,2048]{2,1,0:T(8,128)(2,1)}, bf16[2,8,512]{2,1,0:T(8,128)(2,1)}, f32[8,128]{1,0:T(8,128)}, bf16[4,8,1024]{2,1,0:T(8,128)(2,1)}) custom-call(bf16[8,2048]{1,0:T(8,128)(2,1)} %fusion.32.normed_ref, bf16[4,8,1024]{2,1,0:T(8,128)(2,1)} %get-tuple-element.15.old_ref, bf16[2,1024]{1,0:T(2,128)(2,1)} %gain_ref.3, ...), custom_call_target="tpu_custom_call" | custom-call | tf_op jit(solution)/shard_map/pallas_call | solution.py:302
  58.6 0.8 multiply_exponential_fusion
  59.4 0.7 multiply_reduce_fusion.3
  60.2 0.7 fusion.35
  60.9 0.7 pad_maximum_fusion.5
  61.6 0.8 slice_bitcast_fusion.4
  62.5 0.7 pad_maximum_fusion.2
  63.7 5.7 %fusion.1 = f32[8,32,1,64]{3,2,1,0:T(1,128)S(1)} fusion(f32[8,32,128,1]{2,3,1,0:T(1,128)S(1)} %bitcast.136, f32[2,8,32,64,128]{4,3,2,1,0:T(8,128)} %param.23, f32[8,32,128]{2,1,0:T(8,128)S(1)} %get-tuple-element.45, f32[8,32,64]{2,1,0:T(8,128)S(1)} %broadcast_multiply_fusion, f32[8,32]{1,0:T(8,128)S(1)} %get-tuple-element.22), kind=kOutput, calls=%fused_computation.3 | convolution fusion | flops 10485760 | bytes 8782848 | tf_op jit(solution)/shard_map/bhpn,bhn->bhp/dot_general | solution.py:382
  70.1 0.7 fusion.33.normed_ref
  70.8 11.2 %shard_map.176 = bf16[8,1024]{1,0:T(8,128)(2,1)} custom-call(bf16[8,2048]{1,0:T(8,128)(2,1)} %fusion.33.normed_ref, bf16[4,8,1024]{2,1,0:T(8,128)(2,1)} %get-tuple-element.19.old_ref, bf16[2,2048,1024]{2,1,0:T(8,128)(2,1)} %w_out_ref.3), custom_call_target="tpu_custom_call" | custom-call | tf_op jit(solution)/shard_map/pallas_call | solution.py:332
  82.0 13.0 %multiply_add_fusion = f32[2,8,32,64,128]{4,3,2,1,0:T(8,128)} fusion(f32[2,8,32,64,128]{4,3,2,1,0:T(8,128)} %param.23, f32[2,8,32,128]{3,2,1,0:T(8,128)S(1)} %pad_maximum_fusion.1, f32[2,8,32,64]{3,2,1,0:T(8,128)S(1)} %pad_maximum_fusion, f32[2,8,32]{2,1,0:T(8,128)S(1)} %pad_maximum_fusion.8), kind=kLoop, calls=%fused_computation | loop fusion | flops 12582912 | bytes 33949696 | tf_op jit(solution)/shard_map/add | solution.py:433
  (53 shorter events, 3.0 us)
Async XLA Ops:
  6.0 22.0 %copy-start = (bf16[2,8,3,2048]{3,1,2,0:T(8,128)(2,1)S(1)}, bf16[2,8,3,2048]{3,1,2,0:T(8,128)(2,1)}, u32[]{:S(2)}) copy-start(bf16[2,8,3,2048]{3,1,2,0:T(8,128)(2,1)} %param.21) | copy-start | bytes 589828
  25.5 9.3 %copy-start.2 = (bf16[2,8,2048]{2,1,0:T(8,128)(2,1)S(1)}, bf16[2,8,2048]{2,1,0:T(8,128)(2,1)}, u32[]{:S(2)}) copy-start(bf16[2,8,2048]{2,1,0:T(8,128)(2,1)} %get-tuple-element.13) | copy-start | bytes 196612
  35.4 24.8 %copy-start.4 = (bf16[2,8,512]{2,1,0:T(8,128)(2,1)S(1)}, bf16[2,8,512]{2,1,0:T(8,128)(2,1)}, u32[]{:S(2)}) copy-start(bf16[2,8,512]{2,1,0:T(8,128)(2,1)} %get-tuple-element.14) | copy-start | bytes 49156
  58.6 11.5 %copy-start.1 = (bf16[2,8,2048]{2,1,0:T(8,128)(2,1)S(1)}, bf16[2,8,2048]{2,1,0:T(8,128)(2,1)}, u32[]{:S(2)}) copy-start(bf16[2,8,2048]{2,1,0:T(8,128)(2,1)} %get-tuple-element.17) | copy-start | bytes 196612
  82.0 13.0 %copy-start.3 = (bf16[8,1024]{1,0:T(8,128)(2,1)S(1)}, bf16[8,1024]{1,0:T(8,128)(2,1)}, u32[]{:S(2)}) copy-start(bf16[8,1024]{1,0:T(8,128)(2,1)} %shard_map.176) | copy-start | bytes 49156

commit v3 on v2

--- a/solution.py
+++ b/solution.py
@@ -97,7 +97,7 @@
     for role in range(2):
         put(send_small, role * vec_cols, jnp.dot(lhs, w_vec_buf[role], preferred_element_type=F32))
     copies = deal(send_small, recv_small, sems[0], sems[1], "dp", ndp)
-    block = min(cols, 1024)
+    block = min(cols, 512)
     for role in (0, 1):
         target, landing = ((send_gate, recv_gate), (send_val, recv_val))[role]
         load_in[role].wait()

time: 96.6 us -> 96.6 us (level)
  no operation moved by 1% of the time
where the time goes in v3:
time: 96.6 us; the launch traced here: 95.6 us
  Pallas kernels  53.8 us (56%)
  other arithmetic  24.4 us (25%)
  matrix products  11.4 us (12%)
  local copies, waits for them, and re-layouts  5.04 us (5%)
    pallas_call x1, Pallas kernels, middle_call(): pl.pallas_call(functools.partial(middle_kernel, layer, ntp, ndp), out_sha...  23.2 us
    pallas_call x1, Pallas kernels, first_call(): pl.pallas_call(functools.partial(first_kernel, ntp, ndp), out_shape=(jax....  19.5 us
    add x1, other arithmetic, shards(): decays[..., None, None] * ssm_state  13 us
    dot_general x2, matrix products, head_step(): jnp.einsum('bhpn,bhn->bhp', state, out_vec)  11.4 us
    pallas_call x1, Pallas kernels, last_call(): pl.pallas_call(functools.partial(last_kernel, layer, ntp, ndp), out_shape...  11.2 us
    another operation x4, other arithmetic, shards(): return (current, jnp.stack(convs), jnp.stack(vec_rows), new_ssm)  2.1 us

profile of v3, /device:TPU:0, one launch (start us, length us, event | category | flops | bytes accessed | tf_op | source)
XLA Modules:
  0.0 95.6 jit_solution(13292287167607434752)
XLA Ops:
  0.6 0.8 slice_bitcast_fusion.9
  1.4 0.8 exponential_bitcast_fusion
  2.2 0.8 slice_bitcast_fusion.8
  2.9 0.8 slice_convert_fusion.2
  3.7 0.7 bitcast_convert_fusion.2
  4.4 0.7 bitcast_convert_fusion
  5.2 0.8 slice_bitcast_fusion.2
  6.0 19.5 %shard_map.174 = (bf16[2,8,2048]{2,1,0:T(8,128)(2,1)}, bf16[2,8,512]{2,1,0:T(8,128)(2,1)}, f32[8,128]{1,0:T(8,128)}, bf16[4,8,1024]{2,1,0:T(8,128)(2,1)}) custom-call(bf16[8,1024]{1,0:T(8,128)(2,1)} %x_ref.1, bf16[2,1024]{1,0:T(2,128)(2,1)} %gain_ref.3, bf16[2,1024,128]{2,1,0:T(8,128)(2,1)} %w_step_ref.3, bf16[2,2,1024,2048]{3,2,1,0:T(8,128)(2,1)} %w_in_ref.3, ...), custom_call_target="tpu_custom_call" | custom-call | tf_op jit(solution)/shard_map/pallas_call | solution.py:278
  25.5 0.8 multiply_exponential_fusion.1
  26.3 0.7 multiply_reduce_fusion.5
  27.1 0.8 slice_bitcast_fusion.5
  28.4 5.7 %fusion.4 = f32[8,32,1,64]{3,2,1,0:T(1,128)S(1)} fusion(f32[8,32,128,1]{2,3,1,0:T(1,128)S(1)} %bitcast.137, f32[2,8,32,64,128]{4,3,2,1,0:T(8,128)} %param.23, f32[8,32,128]{2,1,0:T(8,128)S(1)} %get-tuple-element.43, f32[8,32,64]{2,1,0:T(8,128)S(1)} %broadcast_multiply_fusion.1, f32[8,32]{1,0:T(8,128)S(1)} %get-tuple-element.26), kind=kOutput, calls=%fused_computation.6 | convolution fusion | flops 10485760 | bytes 8782848 | tf_op jit(solution)/shard_map/bhpn,bhn->bhp/dot_general | solution.py:382
  34.7 0.7 fusion.32.normed_ref
  35.4 23.2 %shard_map.175 = (bf16[2,8,2048]{2,1,0:T(8,128)(2,1)}, bf16[2,8,512]{2,1,0:T(8,128)(2,1)}, f32[8,128]{1,0:T(8,128)}, bf16[4,8,1024]{2,1,0:T(8,128)(2,1)}) custom-call(bf16[8,2048]{1,0:T(8,128)(2,1)} %fusion.32.normed_ref, bf16[4,8,1024]{2,1,0:T(8,128)(2,1)} %get-tuple-element.15.old_ref, bf16[2,1024]{1,0:T(2,128)(2,1)} %gain_ref.3, ...), custom_call_target="tpu_custom_call" | custom-call | tf_op jit(solution)/shard_map/pallas_call | solution.py:302
  58.6 0.8 multiply_exponential_fusion
  59.4 0.7 multiply_reduce_fusion.3
  60.2 0.7 fusion.35
  60.9 0.7 pad_maximum_fusion.5
  61.6 0.8 slice_bitcast_fusion.4
  62.5 0.7 pad_maximum_fusion.2
  63.7 5.7 %fusion.1 = f32[8,32,1,64]{3,2,1,0:T(1,128)S(1)} fusion(f32[8,32,128,1]{2,3,1,0:T(1,128)S(1)} %bitcast.136, f32[2,8,32,64,128]{4,3,2,1,0:T(8,128)} %param.23, f32[8,32,128]{2,1,0:T(8,128)S(1)} %get-tuple-element.45, f32[8,32,64]{2,1,0:T(8,128)S(1)} %broadcast_multiply_fusion, f32[8,32]{1,0:T(8,128)S(1)} %get-tuple-element.22), kind=kOutput, calls=%fused_computation.3 | convolution fusion | flops 10485760 | bytes 8782848 | tf_op jit(solution)/shard_map/bhpn,bhn->bhp/dot_general | solution.py:382
  70.1 0.7 fusion.33.normed_ref
  70.8 11.2 %shard_map.176 = bf16[8,1024]{1,0:T(8,128)(2,1)} custom-call(bf16[8,2048]{1,0:T(8,128)(2,1)} %fusion.33.normed_ref, bf16[4,8,1024]{2,1,0:T(8,128)(2,1)} %get-tuple-element.19.old_ref, bf16[2,2048,1024]{2,1,0:T(8,128)(2,1)} %w_out_ref.3), custom_call_target="tpu_custom_call" | custom-call | tf_op jit(solution)/shard_map/pallas_call | solution.py:332
  82.0 13.0 %multiply_add_fusion = f32[2,8,32,64,128]{4,3,2,1,0:T(8,128)} fusion(f32[2,8,32,64,128]{4,3,2,1,0:T(8,128)} %param.23, f32[2,8,32,128]{3,2,1,0:T(8,128)S(1)} %pad_maximum_fusion.1, f32[2,8,32,64]{3,2,1,0:T(8,128)S(1)} %pad_maximum_fusion, f32[2,8,32]{2,1,0:T(8,128)S(1)} %pad_maximum_fusion.8), kind=kLoop, calls=%fused_computation | loop fusion | flops 12582912 | bytes 33949696 | tf_op jit(solution)/shard_map/add | solution.py:433
  (53 shorter events, 3.0 us)
Async XLA Ops:
  6.0 22.0 %copy-start = (bf16[2,8,3,2048]{3,1,2,0:T(8,128)(2,1)S(1)}, bf16[2,8,3,2048]{3,1,2,0:T(8,128)(2,1)}, u32[]{:S(2)}) copy-start(bf16[2,8,3,2048]{3,1,2,0:T(8,128)(2,1)} %param.21) | copy-start | bytes 589828
  25.5 9.3 %copy-start.2 = (bf16[2,8,2048]{2,1,0:T(8,128)(2,1)S(1)}, bf16[2,8,2048]{2,1,0:T(8,128)(2,1)}, u32[]{:S(2)}) copy-start(bf16[2,8,2048]{2,1,0:T(8,128)(2,1)} %get-tuple-element.13) | copy-start | bytes 196612
  35.4 24.8 %copy-start.4 = (bf16[2,8,512]{2,1,0:T(8,128)(2,1)S(1)}, bf16[2,8,512]{2,1,0:T(8,128)(2,1)}, u32[]{:S(2)}) copy-start(bf16[2,8,512]{2,1,0:T(8,128)(2,1)} %get-tuple-element.14) | copy-start | bytes 49156
  58.6 11.5 %copy-start.1 = (bf16[2,8,2048]{2,1,0:T(8,128)(2,1)S(1)}, bf16[2,8,2048]{2,1,0:T(8,128)(2,1)}, u32[]{:S(2)}) copy-start(bf16[2,8,2048]{2,1,0:T(8,128)(2,1)} %get-tuple-element.17) | copy-start | bytes 196612
  82.0 13.0 %copy-start.3 = (bf16[8,1024]{1,0:T(8,128)(2,1)S(1)}, bf16[8,1024]{1,0:T(8,128)(2,1)}, u32[]{:S(2)}) copy-start(bf16[8,1024]{1,0:T(8,128)(2,1)} %shard_map.176) | copy-start | bytes 49156
